TPU v7x, 32 devices: a whole 2x2x4 slice. The times are simulated.
32 devices in a mesh: sp: 8 (over z, y), tp: 4 (over x, core).
Axes of the slice: x: 2, y: 2, z: 4, core: 2. Of those that a mesh axis runs over, the one named last changes fastest.
Arguments:
- mixer_output_stream: bfloat16 [1024, 2048], P('sp', 'tp'), may hold values from -6 to 6
- layer_output_gradient: bfloat16 [1024, 2048], P('sp', 'tp'), may hold values from -2.5 to 2.5
- routes: int32 [1024, 2], P('sp'), may hold values from 0 to 7, all different within a row; in each aligned block of 128 rows (0 to 127, 128 to 255, ...) at most 48 rows name the same one
- expert_combine_weight: float32 [1024, 2], P('sp'), may hold values from 0.2 to 1
- expert_gate_weight: bfloat16 [8, 2048, 3584], P('sp', None, 'tp'), may hold values from -0.125 to 0.125
- expert_up_weight: bfloat16 [8, 2048, 3584], P('sp', None, 'tp'), may hold values from -0.125 to 0.125
- expert_down_weight: bfloat16 [8, 3584, 2048], P('sp', 'tp'), may hold values from -0.09375 to 0.09375
- head_mixer_input: bfloat16 [1024, 4096], P('sp', 'tp'), may hold values from -6 to 6
- head_step_size: float32 [1024, 64], P('sp', 'tp'), may hold values from 0.25 to 4
- head_decay_rate: float32 [64], P('tp'), may hold values from 0 to 1
- extra_log_decay: float32 [1024, 64], P('sp', 'tp'), may hold values from -3 to 0
- state_entering_span: float32 [64, 64, 128], P('tp'), may hold values from -48 to 48
- state_input_vectors: bfloat16 [1024, 1024], P('sp', 'tp'), may hold values from -1.75 to 1.75
- state_readout_vectors: bfloat16 [1024, 1024], P('sp', 'tp'), may hold values from -1.75 to 1.75
- gate_preactivation: bfloat16 [1024, 4096], P('sp', 'tp'), may hold values from -6 to 6
- group_norm_scale: float32 [4096], P('tp'), may hold values from 0.1 to 1.9
- mixer_output_weight: bfloat16 [4096, 2048], P('tp', 'sp'), may hold values from -0.09375 to 0.09375
Outputs:
- grad_gate: bfloat16 [8, 2048, 3584], P('sp', None, 'tp')
- grad_up: bfloat16 [8, 2048, 3584], P('sp', None, 'tp')
- grad_down: bfloat16 [8, 3584, 2048], P('sp', 'tp')
- grad_out_proj: float32 [4096, 2048], P('tp', 'sp')
- grad_input: bfloat16 [1024, 4096], P('sp', 'tp')
- grad_step: float32 [1024, 64], P('sp', 'tp')
- grad_state_in: bfloat16 [1024, 1024], P('sp', 'tp')
- grad_read_out: bfloat16 [1024, 1024], P('sp', 'tp')
- grad_gate_in: bfloat16 [1024, 4096], P('sp', 'tp')
Inputs may be any that keep to these rules, and one draw needn't show every extreme that they name: `routes`: the two experts of a token differ. In each aligned block of 128 rows no expert is named more than 48 times, and in every draw some expert is named exactly 48 times in some block.
All inputs are finite; a program needn't handle non-finite values.
Results may differ from a plain program's by a relative error of at most 0.02.
Values may be sent and summed in bfloat16 or wider, within the bound.
A program may use at most 128 MiB of HBM per device.

v0:
```python
import functools

import jax
import jax.numpy as jnp
from jax import lax
from jax.experimental import pallas as pl
from jax.experimental.pallas import tpu as pltpu
from jax.sharding import PartitionSpec as P

HDIM = 64
STATE = 128
BLK = 128


norm_eps = 1e-05
exact_mode = lax.Precision.HIGH


MESH = pl.DeviceIdType.MESH
BF16 = jnp.bfloat16
F32 = jnp.float32
DMA = pltpu.SemaphoreType.DMA


class Place:
    def __init__(self, n_sp, n_tp):
        self.n_sp, self.n_tp = n_sp, n_tp
        self.inner = 2 if n_tp % 2 == 0 else 1
        self.outer = n_tp // self.inner
        self.me = lax.axis_index("sp")
        self.t = lax.axis_index("tp")
        self.core = lax.rem(self.t, self.inner)
        self.far = lax.div(self.t, self.inner)

    def span(self, d):
        return lax.rem(self.me + d, self.n_sp)

    def span_back(self, d):
        return lax.rem(self.me + (self.n_sp - d), self.n_sp)

    def partners(self):
        return [self.far * self.inner + lax.rem(self.core + i, self.inner) for i in range(1, self.inner)]

    def outers(self):
        return [lax.rem(self.far + j, self.outer) * self.inner + self.core for j in range(1, self.outer)]

    def enter(self, with_span=True):
        barrier = pltpu.get_barrier_semaphore()
        devices = [(self.me, p) for p in self.partners() + self.outers()]
        if with_span:
            devices += [(self.span(d), self.t) for d in range(1, self.n_sp)]
        for device in devices:
            pl.semaphore_signal(barrier, inc=1, device_id=device, device_id_type=MESH)
        pl.semaphore_wait(barrier, len(devices))


def remote(src, dst, send, recv, device):
    return pltpu.make_async_remote_copy(
        src_ref=src, dst_ref=dst, send_sem=send, recv_sem=recv, device_id=device, device_id_type=MESH
    )


def decay_column(row, per):
    width = row.shape[-1]
    down = lax.broadcasted_iota(jnp.int32, (per, width), 0)
    across = lax.broadcasted_iota(jnp.int32, (per, width), 1)
    spread = jnp.broadcast_to(row.astype(F32), (per, width))
    return jnp.sum(jnp.where(down == across, spread, 0.0), axis=1, keepdims=True)


def whole(count):
    return [pl.BlockSpec(memory_space=pltpu.VMEM)] * count


HIGHEST = lax.Precision.HIGHEST


def mm(x, y, xd=1, yd=0, precision=None):
    return lax.dot_general(
        x, y, (((xd,), (yd,)), ((), ())), precision=precision, preferred_element_type=F32
    )


def lower_ones(size):
    down = lax.broadcasted_iota(jnp.int32, (size, size), 0)
    across = lax.broadcasted_iota(jnp.int32, (size, size), 1)
    return down >= across


def head_ones(heads, channels):
    down = lax.broadcasted_iota(jnp.int32, (heads, channels), 0)
    across = lax.broadcasted_iota(jnp.int32, (heads, channels), 1)
    return jnp.where(lax.div(across, HDIM) == down, 1.0, 0.0).astype(F32)


def turned(x):
    size = x.shape[1]
    down = lax.broadcasted_iota(jnp.int32, (size, size), 0)
    across = lax.broadcasted_iota(jnp.int32, (size, size), 1)
    return mm(jnp.where(down == across, 1.0, 0.0).astype(F32), x, 1, 1, HIGHEST)


def log_decay_sums(step_ref, rate_ref, extra_ref):
    heads, tokens = step_ref.shape
    log_decay = extra_ref[...] - step_ref[...] * decay_column(rate_ref[...], heads)
    lower = jnp.where(lower_ones(tokens), 1.0, 0.0).astype(F32)
    down = mm(lower, log_decay, 1, 1, HIGHEST)
    across = mm(log_decay, lower, 1, 1, HIGHEST)
    return down, across


def head_decay(down, across, head, mask):
    gap = down[:, head : head + 1] - across[head : head + 1, :]
    return jnp.where(mask, jnp.exp(jnp.where(mask, gap, 0.0)), 0.0)


def group_inverse(gated, group, width):
    part = gated[:, group * width : (group + 1) * width]
    return lax.rsqrt(jnp.mean(part * part, axis=1, keepdims=True) + norm_eps)


def ring_origin(position, count):
    position = lax.rem(position + 2 * count, count)
    return jnp.where(2 * position < count, 2 * position, 2 * count - 1 - 2 * position)


def ring_position(me, count):
    half = lax.div(me, 2)
    return jnp.where(lax.rem(me, 2) == 0, half, count - 1 - half)


class Circle:
    def __init__(self, at, own, slots, sends, recvs, waits):
        self.at, self.own, self.slots = at, own, slots
        self.sends, self.recvs, self.waits = sends, recvs, waits
        self.half = at.n_sp // 2
        self.position = ring_position(at.me, at.n_sp)
        self.after = ring_origin(self.position + 1, at.n_sp)
        self.prior = ring_origin(self.position - 1, at.n_sp)
        self.step = 0

    def block(self, slot):
        return self.own if slot == 0 else self.slots.at[slot]

    def origin(self, slot):
        shift = -slot if slot <= self.half else slot - self.half
        return ring_origin(self.position + shift, self.at.n_sp)

    def part(self, block, p):
        size = self.own.shape[0] // 2
        return block.at[pl.ds(p * size, size)]

    def send(self, source, slot, p, peer):
        copy = remote(
            self.part(source, p),
            self.part(self.slots.at[slot], p),
            self.sends.at[slot, p],
            self.recvs.at[slot, p],
            (peer, self.at.t),
        )
        copy.start()
        self.waits.append(copy.wait_send)

    def landed(self, slot, p):
        block = self.part(self.slots.at[slot], p)
        pltpu.make_async_copy(block, block, self.recvs.at[slot, p]).wait()

    def advance(self):
        half, step = self.half, self.step
        self.step = step + 1
        front, rear = self.block(step), self.block(half + step if step else 0)
        for p in range(2):
            if step and step <= half:
                self.landed(step, p)
            if step and step < half:
                self.landed(half + step, p)
            if step + 1 < half:
                self.send(front, step + 1, p, self.after)
                self.send(rear, half + step + 1, p, self.prior)
            elif step + 1 == half and p == 0:
                self.send(front, half, p, self.after)
            elif step + 1 == half:
                self.send(rear, half, p, self.prior)
        if step == 0:
            return [0]
        return [step, half + step] if step < half else [step]

    def more(self):
        return self.step <= self.half


def main_kernel(
    n_sp,
    n_tp,
    stream_ref,
    own_grad_ref,
    routes_ref,
    combine_ref,
    wg_hbm,
    wu_hbm,
    wd_hbm,
    entering_ref,
    x_ref,
    step_ref,
    rate_ref,
    extra_ref,
    b_ref,
    c_ref,
    z_ref,
    scale_ref,
    out_w_ref,
    rows_t_hbm,
    sent_hbm,
    hidden_t_hbm,
    gate_grad_hbm,
    up_grad_hbm,
    proj_ref,
    dx_ref,
    dstep_ref,
    db_ref,
    dc_ref,
    dgate_ref,
    rows,
    sent,
    rows_t,
    hidden_ref,
    hidden_t,
    gate_grad_ref,
    up_grad_ref,
    rows_out,
    sent_out,
    pick_ref,
    state_out,
    state_in,
    lines_out,
    lines_in,
    span_send,
    tp_send,
    tp_fwd_send,
    block_recv,
    state_send,
    state_recv,
    lines_send,
    lines_recv,
    save_sem,
    wg,
    wu,
    wd,
    acc_gate,
    acc_up,
    acc_down,
    part,
    pair_in,
    far_out,
    far_in,
    ret_out,
    ret_in,
    before_tmp,
    before_in,
    mix_own,
    mix,
    mix_parts,
    mix_cols,
    w_slots,
    norm_own,
    norm_slots,
    y_ref,
    total_ref,
    scaled_ref,
    grown_ref,
    ends_ref,
    g_ref,
    sgrad_ref,
    dbp_ref,
    moved_ref,
    reached_ref,
    reached_in,
    after_tmp,
    later_in,
    load_sem,
    pair_send,
    pair_recv,
    far_send,
    far_recv,
    ret_send,
    ret_recv,
    mix_send,
    mix_recv,
    back_send,
    back_recv,
    w_send,
    w_recv,
    norm_send,
    norm_recv,
    reach_send,
    reach_recv,
    later_send,
    later_recv,
    cols_send,
    near_send,
    fwd_send,
    cols_recv,
):
    at = Place(n_sp, n_tp)
    me, t = at.me, at.t
    width = own_grad_ref.shape[1]
    _, capacity, model_width = rows.shape
    pairs = n_sp * capacity
    tokens, channels = x_ref.shape
    per = channels // n_sp
    heads = step_ref.shape[0]
    groups = b_ref.shape[1] // STATE
    group_width = channels // groups
    waits = []

    def cols(owner):
        return pl.ds(pl.multiple_of(owner * width, width), width)

    def landed(block, sem):
        pltpu.make_async_copy(block, block, sem).wait()

    def push(source, target, send, recv, device):
        copy = remote(source, target, send, recv, device)
        copy.start()
        waits.append(copy.wait_send)

    loads = []
    for i, (source, target) in enumerate(((wg_hbm, wg), (wu_hbm, wu), (wd_hbm, wd))):
        loads.append(pltpu.make_async_copy(source, target, load_sem.at[i]))
        loads[-1].start()
    at.enter()
    w_ring = Circle(at, out_w_ref, w_slots, w_send, w_recv, waits)
    norm_ring = Circle(at, norm_own, norm_slots, norm_send, norm_recv, waits)
    w_ring.advance()

    routes = turned(routes_ref[...].astype(F32))
    combine = turned(combine_ref[...])
    top = routes.shape[1]
    expert_lane = lax.broadcasted_iota(jnp.int32, (tokens, n_sp), 1).astype(F32)
    slot_lane = lax.broadcasted_iota(jnp.int32, (tokens, capacity), 1).astype(F32)
    mask = lower_ones(tokens)
    named = [routes[:, k : k + 1] == expert_lane for k in range(top)]
    ones = sum(jnp.where(n, 1.0, 0.0) for n in named)
    earlier = mm(jnp.where(mask, 1.0, 0.0).astype(BF16), ones.astype(BF16)) - ones
    weighted = [
        (own_grad_ref[...].astype(F32) * combine[:, k : k + 1]).astype(BF16) for k in range(top)
    ]
    places = [jnp.sum(jnp.where(n, earlier, 0.0), axis=1, keepdims=True) for n in named]
    for e in range(n_sp):
        picks = []
        for k in range(top):
            place = jnp.where(routes[:, k : k + 1] == float(e), places[k], -1.0)
            picks.append(jnp.where(place == slot_lane, 1.0, 0.0).astype(BF16))
        pick = sum(picks)
        pick_ref[e] = pick
        rows_out[e] = mm(pick, stream_ref[...], 0, 0).astype(BF16)
        sent_out[e] = sum(mm(p, w, 0, 0) for p, w in zip(picks, weighted)).astype(BF16)
    both = ((rows_out, rows), (sent_out, sent))
    for d in range(1, n_sp):
        peer = at.span(d)
        for a, (source, target) in enumerate(both):
            push(
                source.at[peer],
                target.at[me, :, cols(t)],
                span_send.at[a, d],
                block_recv.at[a, me, t],
                (peer, t),
            )

    def pass_on(d, sources, peers, owner, sems, base):
        src_span = at.span_back(d)
        for a in range(2):
            for i, peer in enumerate(peers):
                push(
                    sources[a],
                    both[a][1].at[src_span, :, cols(owner)],
                    sems.at[a, d, base + i],
                    block_recv.at[a, src_span, owner],
                    (me, peer),
                )

    def block_landed(a, src_span, owner):
        landed(both[a][1].at[src_span, :, cols(owner)], block_recv.at[a, src_span, owner])

    near = at.outers() + at.partners()
    pass_on(0, [rows_out.at[me], sent_out.at[me]], near, t, tp_send, 0)
    rows[me, :, cols(t)] = rows_out[me]
    sent[me, :, cols(t)] = sent_out[me]

    down, across = log_decay_sums(step_ref, rate_ref, extra_ref)
    wide = head_ones(heads, channels)
    lane = lax.broadcasted_iota(jnp.int32, (tokens, 2 * HDIM), 1)
    step_wide = mm(turned(step_ref[...]), wide, precision=HIGHEST)
    scaled_ref[...] = x_ref[...].astype(F32) * step_wide
    down_wide = mm(down, wide, precision=HIGHEST)
    grown_ref[...] = jnp.exp(down_wide)
    ends_ref[...] = jnp.exp(down_wide[tokens - 1 : tokens, :] - down_wide)
    spans = n_sp // groups
    for g in range(groups):
        lanes = slice(g * group_width, (g + 1) * group_width)
        left = (scaled_ref[:, lanes] * ends_ref[:, lanes]).astype(BF16)
        state = mm(left, b_ref[:, g * STATE : (g + 1) * STATE], 0, 0).astype(BF16)
        state_out[g * spans : (g + 1) * spans] = state.reshape(spans, per, STATE)
    whole_decay = jnp.exp(down_wide[tokens - 1 : tokens, :])
    lines_out[...] = jnp.zeros(lines_out.shape, BF16)
    for k in range(n_sp):
        lines_out[k, :, :per] = whole_decay[:, k * per : (k + 1) * per].astype(BF16)
    for d in range(1, n_sp):
        peer = at.span(d)
        push(state_out.at[peer], state_in.at[me], state_send.at[d], state_recv.at[me], (peer, t))
        push(lines_out.at[peer], lines_in.at[me], lines_send.at[d], lines_recv.at[me], (peer, t))
    state_in[me] = state_out[me]
    lines_in[me] = lines_out[me]

    for d in range(1, n_sp):
        src_span = at.span_back(d)
        for a in range(2):
            block_landed(a, src_span, t)
        pass_on(d, [b[1].at[src_span, :, cols(t)] for b in both], near, t, tp_send, 0)
    for d in range(n_sp):
        src_span = at.span_back(d)
        for j, owner in enumerate(at.outers()):
            for a in range(2):
                block_landed(a, src_span, owner)
            pass_on(
                d,
                [b[1].at[src_span, :, cols(owner)] for b in both],
                at.partners(),
                owner,
                tp_fwd_send,
                j * (at.inner - 1),
            )
    for d in range(1, n_sp):
        src_span = at.span_back(d)
        landed(state_in.at[src_span], state_recv.at[src_span])
        landed(lines_in.at[src_span], lines_recv.at[src_span])
    running = entering_ref[pl.ds(pl.multiple_of(me * per, per), per), :]
    for k in range(n_sp):
        before_tmp[k] = running.astype(BF16)
        running = decay_column(lines_in[k], per) * running + state_in[k].astype(F32)
    for d in range(1, n_sp):
        peer = at.span(d)
        push(before_tmp.at[peer], before_in.at[me], back_send.at[d], back_recv.at[me], (peer, t))
    before_in[me] = before_tmp[me]
    w_there = [0] + w_ring.advance()
    for d in range(n_sp):
        src_span = at.span_back(d)
        for partner in at.partners():
            core = lax.rem(partner, at.inner)
            for far in range(at.outer):
                for a in range(2):
                    block_landed(a, src_span, far * at.inner + core)

    saves = []

    def save(source, target):
        copy = pltpu.make_async_copy(source, target, save_sem.at[len(saves)])
        copy.start()
        saves.append(copy)

    save(sent, sent_hbm)

    deep = 256

    def chunk(i):
        return pl.ds(pl.multiple_of(i * deep, deep), deep)

    acc_gate[...] = jnp.zeros(acc_gate.shape, F32)
    acc_up[...] = jnp.zeros(acc_up.shape, F32)
    acc_down[...] = jnp.zeros(acc_down.shape, F32)
    loads[0].wait()

    @pl.loop(0, model_width // deep)
    def _(i):
        acc_gate[...] += mm(rows[:, :, chunk(i)].reshape(pairs, deep), wg[chunk(i), :])

    loads[1].wait()

    @pl.loop(0, model_width // deep)
    def _(i):
        acc_up[...] += mm(rows[:, :, chunk(i)].reshape(pairs, deep), wu[chunk(i), :])

    loads[2].wait()

    @pl.loop(0, model_width // deep)
    def _(i):
        acc_down[...] += mm(sent[:, :, chunk(i)].reshape(pairs, deep), wd[:, chunk(i)], 1, 1)

    @pl.loop(0, n_sp)
    def _(i):
        piece = pl.ds(pl.multiple_of(i * capacity, capacity), capacity)
        pre_gate, pre_up, hidden_grad = acc_gate[piece, :], acc_up[piece, :], acc_down[piece, :]
        gate = jax.nn.sigmoid(pre_gate)
        silu = pre_gate * gate
        hidden_ref[piece, :] = (silu * pre_up).astype(BF16)
        slope = gate * (1.0 + pre_gate * (1.0 - gate))
        gate_grad_ref[piece, :] = (hidden_grad * pre_up * slope).astype(BF16)
        up_grad_ref[piece, :] = (hidden_grad * silu).astype(BF16)

    order = list(range(1, n_sp)) + [0]
    fars = list(range(1, at.outer)) + [0]

    def partial_columns(owner):
        rows = cols(owner)
        value = mm(gate_grad_ref[...], wg[rows, :], 1, 1) + mm(up_grad_ref[...], wu[rows, :], 1, 1)
        part[:, :, rows] = value.astype(BF16).reshape(n_sp, capacity, width)

    for i, partner in enumerate(at.partners()):
        core = lax.rem(partner, at.inner)
        for j in fars:
            far = lax.rem(at.far + j, at.outer)
            owner = far * at.inner + core
            partial_columns(owner)
            for d in order:
                span = at.span(d)
                push(
                    part.at[span, :, cols(owner)],
                    pair_in.at[i, j, span],
                    pair_send.at[i, j, d],
                    pair_recv.at[i, j, span],
                    (me, partner),
                )
    for j in fars:
        partial_columns(lax.rem(at.far + j, at.outer) * at.inner + at.core)

    def pair_sum(span, j):
        far = lax.rem(at.far + j, at.outer)
        value = part[span, :, cols(far * at.inner + at.core)].astype(F32)
        for i in range(at.inner - 1):
            value = value + pair_in[i, j, span].astype(F32)
        return value

    for d in order:
        span = at.span(d)
        for j in fars:
            for i in range(at.inner - 1):
                landed(pair_in.at[i, j, span], pair_recv.at[i, j, span])
            if j:
                far_out[j - 1, span] = pair_sum(span, j).astype(BF16)
                push(
                    far_out.at[j - 1, span],
                    far_in.at[j - 1, span],
                    far_send.at[j - 1, d],
                    far_recv.at[j - 1, span],
                    (me, lax.rem(at.far + j, at.outer) * at.inner + at.core),
                )
    w_there += w_ring.advance()
    save(gate_grad_ref, gate_grad_hbm)
    save(up_grad_ref, up_grad_hbm)

    for d in range(1, n_sp):
        src_span = at.span_back(d)
        landed(before_in.at[src_span], back_recv.at[src_span])
    before_rows = before_in[...].reshape(n_sp * per, STATE)
    for g in range(groups):
        states = slice(g * STATE, (g + 1) * STATE)
        lanes = slice(g * group_width, (g + 1) * group_width)
        b_rows, c_rows = b_ref[:, states], c_ref[:, states]
        affinity = mm(c_rows, b_rows, 1, 1)
        off = mm(c_rows, before_rows[lanes], 1, 1) * grown_ref[:, lanes]
        pieces = []
        for pair in range(group_width // (2 * HDIM)):
            first = g * group_width + pair * 2 * HDIM
            head = first // HDIM
            values = scaled_ref[:, first : first + 2 * HDIM].astype(BF16)
            left = mm((affinity * head_decay(down, across, head, mask)).astype(BF16), values)
            right = mm((affinity * head_decay(down, across, head + 1, mask)).astype(BF16), values)
            pieces.append(jnp.where(lane < HDIM, left, right))
        y = jnp.concatenate(pieces, axis=1) + off
        y_ref[:, lanes] = y
        z = z_ref[:, lanes].astype(F32)
        gated = y * (z * jax.nn.sigmoid(z))
        normed = gated * group_inverse(gated, 0, group_width) * scale_ref[:, lanes]
        norm_own[lanes] = normed.T.astype(BF16)

    for d in order:
        span = at.span(d)
        value = pair_sum(span, 0)
        for j in range(1, at.outer):
            landed(far_in.at[j - 1, span], far_recv.at[j - 1, span])
            value = value + far_in[j - 1, span].astype(F32)
        if d == 0:
            ret_in[me] = value.astype(BF16)
        else:
            ret_out[span] = value.astype(BF16)
            push(ret_out.at[span], ret_in.at[me], ret_send.at[d], ret_recv.at[me], (span, t))
    w_there += w_ring.advance()
    value = own_grad_ref[...].astype(F32)
    value = value + mm(pick_ref[me], ret_in[me])
    for d in range(1, n_sp):
        span = at.span_back(d)
        landed(ret_in.at[span], ret_recv.at[span])
        value = value + mm(pick_ref[span], ret_in[span])
    mix_own[...] = value.astype(BF16)
    mix[:, cols(t)] = value.astype(BF16)
    for i, peer in enumerate(near):
        push(mix_own, mix.at[:, cols(t)], mix_send.at[0, i], mix_recv.at[t], (me, peer))
    for j, owner in enumerate(at.outers()):
        block = mix.at[:, cols(owner)]
        landed(block, mix_recv.at[owner])
        for i, partner in enumerate(at.partners()):
            push(block, block, mix_send.at[1 + j, i], mix_recv.at[owner], (me, partner))
    for partner in at.partners():
        core = lax.rem(partner, at.inner)
        for far in range(at.outer):
            owner = far * at.inner + core
            landed(mix.at[:, cols(owner)], mix_recv.at[owner])
    part_width = model_width // n_sp
    for k in range(n_sp):
        mix_parts[k] = mix[:, k * part_width : (k + 1) * part_width]

    total_ref[...] = jnp.zeros(total_ref.shape, F32)
    while True:
        for slot in w_there:
            total_ref[...] += mm(mix_parts[w_ring.origin(slot)], w_ring.block(slot)[...], 1, 1)
        if not w_ring.more():
            break
        w_there = w_ring.advance()
    norm_ring.advance()
    for g in range(groups):
        lanes = slice(g * group_width, (g + 1) * group_width)
        y, z = y_ref[:, lanes], z_ref[:, lanes].astype(F32)
        gate = jax.nn.sigmoid(z)
        silu = z * gate
        gated = y * silu
        inverse = group_inverse(gated, 0, group_width)
        unit = gated * inverse
        grad = total_ref[:, lanes] * scale_ref[:, lanes]
        grad = inverse * (grad - unit * jnp.mean(grad * unit, axis=1, keepdims=True))
        dgate_ref[:, lanes] = (grad * y * gate * (1.0 + z * (1.0 - gate))).astype(BF16)
        scan_grad = grad * silu
        g_ref[:, lanes] = scan_grad
        weighted = (scan_grad * grown_ref[:, lanes]).astype(BF16)
        reached = mm(weighted, c_ref[:, g * STATE : (g + 1) * STATE], 0, 0).astype(BF16)
        share = n_sp // groups
        reached_ref[g * share : (g + 1) * share] = reached.reshape(share, per, STATE)
    for d in range(1, n_sp):
        peer = at.span(d)
        push(reached_ref.at[peer], reached_in.at[me], reach_send.at[d], reach_recv.at[me], (peer, t))
    reached_in[me] = reached_ref[me]

    head_lane = lax.broadcasted_iota(jnp.int32, (tokens, heads), 1)
    head_down = lax.broadcasted_iota(jnp.int32, (heads, tokens), 0)
    sums = jnp.zeros((tokens, heads), F32)
    column_sums = jnp.zeros((heads, tokens), F32)
    for g in range(groups):
        states = slice(g * STATE, (g + 1) * STATE)
        lanes = slice(g * group_width, (g + 1) * group_width)
        b_rows, c_rows = b_ref[:, states], c_ref[:, states]
        affinity = mm(c_rows, b_rows, 1, 1)
        before = before_rows[lanes]
        affinity_grad = jnp.zeros((tokens, tokens), F32)
        for pair in range(group_width // (2 * HDIM)):
            first = g * group_width + pair * 2 * HDIM
            block = slice(first, first + 2 * HDIM)
            values = scaled_ref[:, block].astype(BF16)
            grads = g_ref[:, block].astype(BF16)
            halves = []
            for side in range(2):
                head = first // HDIM + side
                decay = head_decay(down, across, head, mask)
                own = grads * jnp.where((lane < HDIM) == (side == 0), 1.0, 0.0).astype(BF16)
                inner = mm(own, values, 1, 1) * decay
                affinity_grad = affinity_grad + inner
                moved = inner * affinity
                by_row = jnp.sum(moved, axis=1, keepdims=True)
                by_column = jnp.sum(moved, axis=0, keepdims=True)
                sums = sums + jnp.where(head_lane == head, by_row, 0.0)
                column_sums = column_sums + jnp.where(head_down == head, by_column, 0.0)
                halves.append(mm((affinity * decay).astype(BF16), grads, 0, 0))
            sgrad_ref[:, block] = jnp.where(lane < HDIM, halves[0], halves[1])
        grad = g_ref[:, lanes]
        grown = grown_ref[:, lanes]
        total_ref[:, lanes] = grad * (mm(c_rows, before, 1, 1) * grown)
        low = affinity_grad.astype(BF16)
        dc_ref[:, states] = (mm(low, b_rows) + mm((grad * grown).astype(BF16), before)).astype(BF16)
        dbp_ref[:, states] = mm(low, c_rows, 0, 0)
    through = mm(total_ref[...], wide, 1, 1, precision=HIGHEST)
    moved_ref[...] = sums - column_sums.T + through

    for d in range(1, n_sp):
        src_span = at.span_back(d)
        landed(reached_in.at[src_span], reach_recv.at[src_span])
    running = jnp.zeros(reached_ref.shape[1:], F32)
    for k in reversed(range(n_sp)):
        after_tmp[k] = running.astype(BF16)
        column = decay_column(lines_in[k], per)
        running = column * running + reached_in[k].astype(F32)
    for d in range(1, n_sp):
        peer = at.span(d)
        push(after_tmp.at[peer], later_in.at[me], later_send.at[d], later_recv.at[me], (peer, t))
    later_in[me] = after_tmp[me]
    share = tokens // n_tp

    def stripe(owner):
        return pl.ds(pl.multiple_of(owner * share, share), share)

    for d in range(1, n_sp):
        peer = at.span(d)
        push(
            mix_parts.at[peer, stripe(t)],
            mix_cols.at[me, stripe(t)],
            cols_send.at[d],
            cols_recv.at[me, t],
            (peer, t),
        )
    mix_cols[me] = mix_parts[me]
    norm_there = [0] + norm_ring.advance()
    for i in range(model_width // deep):
        piece = slice(i * deep, (i + 1) * deep)
        rows_t[piece] = rows[:, :, piece].reshape(pairs, deep).astype(F32).T.astype(BF16)
    hidden_t[...] = hidden_ref[...].astype(F32).T.astype(BF16)
    save(rows_t, rows_t_hbm)
    save(hidden_t, hidden_t_hbm)
    for d in range(1, n_sp):
        src_span = at.span_back(d)
        landed(later_in.at[src_span], later_recv.at[src_span])
    later_rows = later_in[...].reshape(n_sp * per, STATE)
    carried = []
    for g in range(groups):
        states = slice(g * STATE, (g + 1) * STATE)
        lanes = slice(g * group_width, (g + 1) * group_width)
        b_rows, later = b_ref[:, states], later_rows[lanes]
        ends, scaled = ends_ref[:, lanes], scaled_ref[:, lanes]
        from_later = mm(b_rows, later, 1, 1) * ends
        scaled_grad = sgrad_ref[:, lanes] + from_later
        total_ref[:, lanes] = scaled * from_later
        g_ref[:, lanes] = scaled_grad * x_ref[:, lanes].astype(F32)
        dx_ref[:, lanes] = (scaled_grad * step_wide[:, lanes]).astype(BF16)
        db_ref[:, states] = (dbp_ref[:, states] + mm((scaled * ends).astype(BF16), later)).astype(
            BF16
        )
        both = before_rows[lanes].astype(F32) * later.astype(F32)
        carried.append(jnp.sum(both, axis=1, keepdims=True))
    ended = mm(total_ref[...], wide, 1, 1, precision=HIGHEST)
    stepped = mm(g_ref[...], wide, 1, 1, precision=HIGHEST)
    both = jnp.broadcast_to(jnp.concatenate(carried, axis=0), (channels, STATE))
    carried = mm(jnp.ones((8, STATE), F32), mm(wide, both, precision=HIGHEST), 1, 1, HIGHEST)
    carried = carried[:1] * (1.0 / STATE) * jnp.exp(down[tokens - 1 : tokens, :])
    moved = moved_ref[...] - ended
    final = jnp.sum(ended, axis=0, keepdims=True) + carried
    lower = jnp.where(mask, 1.0, 0.0).astype(F32)
    decay_grad = mm(lower, moved, 0, 0, precision=HIGHEST) + final
    dstep_ref[...] = (stepped - rate_ref[...] * decay_grad).T

    for d in range(1, n_sp):
        src_span = at.span_back(d)
        block = mix_cols.at[src_span, stripe(t)]
        landed(block, cols_recv.at[src_span, t])
        for i, peer in enumerate(near):
            push(block, block, near_send.at[d, i], cols_recv.at[src_span, t], (me, peer))
    norm_there += norm_ring.advance()
    for d in range(1, n_sp):
        src_span = at.span_back(d)
        for j, owner in enumerate(at.outers()):
            block = mix_cols.at[src_span, stripe(owner)]
            landed(block, cols_recv.at[src_span, owner])
            for i, partner in enumerate(at.partners()):
                push(block, block, fwd_send.at[d, j, i], cols_recv.at[src_span, owner], (me, partner))
    for d in range(1, n_sp):
        src_span = at.span_back(d)
        for partner in at.partners():
            core = lax.rem(partner, at.inner)
            for far in range(at.outer):
                owner = far * at.inner + core
                landed(mix_cols.at[src_span, stripe(owner)], cols_recv.at[src_span, owner])
    proj_ref[...] = jnp.zeros(proj_ref.shape, F32)
    while True:
        for slot in norm_there:
            proj_ref[...] += mm(norm_ring.block(slot)[...], mix_cols[norm_ring.origin(slot)])
        if not norm_ring.more():
            break
        norm_there = norm_ring.advance()
    for wait in waits:
        wait()
    for copy in saves:
        copy.wait()


def main_part(stream, own_grad, routes, combine, weights, entering, scan_args, out_weight, n_sp, n_tp):
    tokens, width = own_grad.shape
    model_width, units = weights[0].shape
    capacity = -(-3 * tokens // n_sp)
    capacity = -(-capacity // 16) * 16
    pairs = n_sp * capacity
    x, step, rate, extra, b_rows, c_rows, gate, scale = scan_args
    channels = x.shape[1]
    heads = step.shape[0]
    per, lanes = channels // n_sp, entering.shape[1]
    out_columns = out_weight.shape[1]
    inner = 2 if n_tp % 2 == 0 else 1
    outer = n_tp // inner
    mates, others = max(inner - 1, 1), max(outer - 1, 1)
    near = max(inner + outer - 2, 1)
    blocks = (n_sp, capacity, width)
    states = (n_sp, per, lanes)

    def low(*shape):
        return pltpu.VMEM(shape, BF16)

    def full(*shape):
        return pltpu.VMEM(shape, F32)

    def out(shape, dtype):
        return jax.ShapeDtypeStruct(shape, dtype)

    anywhere = pl.BlockSpec(memory_space=pl.ANY)
    args = (stream, own_grad, routes, combine, *weights, entering, *scan_args, out_weight)
    return pl.pallas_call(
        functools.partial(main_kernel, n_sp, n_tp),
        out_shape=(
            out((model_width, pairs), BF16),
            out((n_sp, capacity, model_width), BF16),
            out((units, pairs), BF16),
            out((pairs, units), BF16),
            out((pairs, units), BF16),
            out((channels, out_columns), F32),
            out(x.shape, BF16),
            out(step.shape, F32),
            out(b_rows.shape, BF16),
            out(c_rows.shape, BF16),
            out(x.shape, BF16),
        ),
        in_specs=whole(4) + [anywhere] * 3 + whole(len(args) - 7),
        out_specs=tuple([anywhere] * 5 + whole(6)),
        scratch_shapes=[
            low(n_sp, capacity, model_width),
            low(n_sp, capacity, model_width),
            low(model_width, pairs),
            low(pairs, units),
            low(units, pairs),
            low(pairs, units),
            low(pairs, units),
            low(*blocks),
            low(*blocks),
            low(n_sp, tokens, capacity),
            low(*states),
            low(*states),
            low(n_sp, 1, lanes),
            low(n_sp, 1, lanes),
            DMA((2, n_sp)),
            DMA((2, n_sp, near)),
            DMA((2, n_sp, max((outer - 1) * (inner - 1), 1))),
            DMA((2, n_sp, n_tp)),
            DMA((n_sp,)),
            DMA((n_sp,)),
            DMA((n_sp,)),
            DMA((n_sp,)),
            DMA((5,)),
            low(model_width, units),
            low(model_width, units),
            low(units, model_width),
            full(pairs, units),
            full(pairs, units),
            full(pairs, units),
            low(n_sp, capacity, model_width),
            low(mates, outer, *blocks),
            low(others, *blocks),
            low(others, *blocks),
            low(*blocks),
            low(*blocks),
            low(*states),
            low(*states),
            low(tokens, width),
            low(tokens, model_width),
            low(n_sp, tokens, out_columns),
            low(n_sp, tokens, out_columns),
            low(n_sp, channels, out_columns),
            low(channels, tokens),
            low(n_sp, channels, tokens),
            full(tokens, channels),
            full(tokens, channels),
            full(tokens, channels),
            full(tokens, channels),
            full(tokens, channels),
            full(tokens, channels),
            full(tokens, channels),
            full(*b_rows.shape),
            full(tokens, heads),
            low(*states),
            low(*states),
            low(*states),
            low(*states),
            DMA((3,)),
            DMA((mates, outer, n_sp)),
            DMA((mates, outer, n_sp)),
            DMA((others, n_sp)),
            DMA((others, n_sp)),
            DMA((n_sp,)),
            DMA((n_sp,)),
            DMA((outer, near)),
            DMA((n_tp,)),
            DMA((n_sp,)),
            DMA((n_sp,)),
            DMA((n_sp, 2)),
            DMA((n_sp, 2)),
            DMA((n_sp, 2)),
            DMA((n_sp, 2)),
            DMA((n_sp,)),
            DMA((n_sp,)),
            DMA((n_sp,)),
            DMA((n_sp,)),
            DMA((n_sp,)),
            DMA((n_sp, near)),
            DMA((n_sp, others, mates)),
            DMA((n_sp, n_tp)),
        ],
        compiler_params=pltpu.CompilerParams(
            collective_id=2, has_side_effects=True, vmem_limit_bytes=67_000_000
        ),
        name="main_part",
    )(*args)


def weight_grad_kernel(count, rows_ref, hidden_ref, sent_ref, gate_ref, up_ref, *rest):
    ready, (g_out, u_out, d_out), out = rest[:count], rest[count : count + 3], rest[count + 3 :]
    capacity = sent_ref.shape[1]
    sent = sent_ref[...].reshape(sent_ref.shape[0] * capacity, sent_ref.shape[2])
    g_out[...] = mm(rows_ref[...], gate_ref[...]).astype(BF16)
    u_out[...] = mm(rows_ref[...], up_ref[...]).astype(BF16)
    d_out[...] = mm(hidden_ref[...], sent).astype(BF16)
    for source, target in zip(ready, out):
        target[...] = source[...]


def expert_weight_grads(rows_t, sent, hidden_t, gate_grad, up_grad, ready):
    model_width, pairs = rows_t.shape
    units = hidden_t.shape[0]
    tile = 512
    steps = model_width // tile
    fixed = pl.BlockSpec((pairs, units), lambda i: (0, 0))
    tall = pl.BlockSpec((tile, units), lambda i: (i, 0))
    handed = []
    for array in ready:
        if array.shape[0] % (16 * steps):
            handed.append(pl.BlockSpec(array.shape, lambda i: (0, 0)))
        else:
            handed.append(pl.BlockSpec((array.shape[0] // steps, array.shape[1]), lambda i: (i, 0)))
    return pl.pallas_call(
        functools.partial(weight_grad_kernel, len(ready)),
        grid=(steps,),
        out_shape=(
            jax.ShapeDtypeStruct((model_width, units), BF16),
            jax.ShapeDtypeStruct((model_width, units), BF16),
            jax.ShapeDtypeStruct((units, model_width), BF16),
            *(jax.ShapeDtypeStruct(array.shape, array.dtype) for array in ready),
        ),
        in_specs=[
            pl.BlockSpec((tile, pairs), lambda i: (i, 0)),
            pl.BlockSpec((units, pairs), lambda i: (0, 0)),
            pl.BlockSpec(sent.shape[:2] + (tile,), lambda i: (0, 0, i)),
            fixed,
            fixed,
            *handed,
        ],
        out_specs=(tall, tall, pl.BlockSpec((units, tile), lambda i: (0, i)), *handed),
        name="expert_weight_grads",
    )(rows_t, hidden_t, sent, gate_grad, up_grad, *ready)


def body(
    mixer_output_stream,
    layer_output_gradient,
    routes,
    expert_combine_weight,
    expert_gate_weight,
    expert_up_weight,
    expert_down_weight,
    head_mixer_input,
    head_step_size,
    head_decay_rate,
    extra_log_decay,
    state_entering_span,
    state_input_vectors,
    state_readout_vectors,
    gate_preactivation,
    group_norm_scale,
    mixer_output_weight,
):
    n_sp, n_tp = lax.axis_size("sp"), lax.axis_size("tp")
    rows_t, sent, hidden_t, gate_grad, up_grad, *ready = main_part(
        mixer_output_stream,
        layer_output_gradient,
        routes.T,
        expert_combine_weight.T,
        (expert_gate_weight[0], expert_up_weight[0], expert_down_weight[0]),
        state_entering_span.reshape(-1, STATE),
        (
            head_mixer_input,
            head_step_size.T,
            head_decay_rate[None, :],
            extra_log_decay.T,
            state_input_vectors,
            state_readout_vectors,
            gate_preactivation,
            group_norm_scale[None, :],
        ),
        mixer_output_weight,
        n_sp,
        n_tp,
    )
    grad_g, grad_u, grad_d, proj_grad, input_grad, step_grad, b_grad, c_grad, gate_grad_in = (
        expert_weight_grads(rows_t, sent, hidden_t, gate_grad, up_grad, ready)
    )
    return (
        grad_g[None],
        grad_u[None],
        grad_d[None],
        proj_grad,
        input_grad,
        step_grad.T,
        b_grad,
        c_grad,
        gate_grad_in,
    )


def solution(mesh):
    return jax.shard_map(
        body,
        mesh=mesh,
        in_specs=(
            P("sp", "tp"),
            P("sp", "tp"),
            P("sp", None),
            P("sp", None),
            P("sp", None, "tp"),
            P("sp", None, "tp"),
            P("sp", "tp", None),
            P("sp", "tp"),
            P("sp", "tp"),
            P("tp"),
            P("sp", "tp"),
            P("tp", None, None),
            P("sp", "tp"),
            P("sp", "tp"),
            P("sp", "tp"),
            P("tp"),
            P("tp", "sp"),
        ),
        out_specs=(
            P("sp", None, "tp"),
            P("sp", None, "tp"),
            P("sp", "tp", None),
            P("tp", "sp"),
            P("sp", "tp"),
            P("sp", "tp"),
            P("sp", "tp"),
            P("sp", "tp"),
            P("sp", "tp"),
        ),
        check_vma=False,
    )
```

profile of v0, /device:TPU:0, one launch (start us, length us, event | category | flops | bytes accessed | tf_op | source)
XLA Modules:
  0.0 146.0 jit_solution(9510319393788505637)
XLA Ops:
  0.6 134.7 %main_part.1 = (bf16[2048,384]{1,0:T(8,128)(2,1)}, bf16[8,48,2048]{2,1,0:T(8,128)(2,1)}, bf16[896,384]{1,0:T(8,128)(2,1)}, bf16[384,896]{1,0:T(8,128)(2,1)}, bf1...) custom-call(bf16[128,512]{1,0:T(8,128)(2,1)} %stream_ref.1, ...), custom_call_target="tpu_custom_call" | custom-call | tf_op jit(solution)/shard_map/main_part/pallas_call | solution.py:809
  135.3 10.5 %expert_weight_grads.1 = (bf16[2048,896]{1,0:T(8,128)(2,1)}, bf16[2048,896]{1,0:T(8,128)(2,1)}, bf16[896,2048]{1,0:T(8,128)(2,1)}, f32[1024,256]{1,0:T(8,128)}, ...) custom-call(bf16[2048,384]{1,0:T(8,128)(2,1)} %get-tuple-element.29., ...), custom_call_target="tpu_custom_call" | custom-call | tf_op jit(solution)/shard_map/expert_weight_grads/pallas_call | solution.py:939
where the time goes:
time: 146 us
  Pallas kernels  145 us (99%)
    pallas_call x1, Pallas kernels, main_part(): pl.pallas_call(functools.partial(main_kernel, n_sp, n_tp), out_shape=(out...  135 us
    pallas_call x1, Pallas kernels, expert_weight_grads(): pl.pallas_call(functools.partial(weight_grad_kernel, len(ready)), grid=(s...  10.5 us

commit v1 on v0

--- a/solution.py
+++ b/solution.py
@@ -210,10 +210,15 @@
     scale_ref,
     out_w_ref,
     rows_t_hbm,
-    sent_hbm,
-    hidden_t_hbm,
+    down_hbm,
     gate_grad_hbm,
     up_grad_hbm,
+    proj_hbm,
+    dx_hbm,
+    dstep_hbm,
+    db_hbm,
+    dc_hbm,
+    dgate_hbm,
     proj_ref,
     dx_ref,
     dstep_ref,
@@ -458,8 +463,6 @@
         copy.start()
         saves.append(copy)
 
-    save(sent, sent_hbm)
-
     deep = 256
 
     def chunk(i):
@@ -678,6 +681,10 @@
     through = mm(total_ref[...], wide, 1, 1, precision=HIGHEST)
     moved_ref[...] = sums - column_sums.T + through
 
+    save(dc_ref, dc_hbm)
+    save(dgate_ref, dgate_hbm)
+    norm_there = [0] + norm_ring.advance()
+
     for d in range(1, n_sp):
         src_span = at.span_back(d)
         landed(reached_in.at[src_span], reach_recv.at[src_span])
@@ -705,13 +712,16 @@
             (peer, t),
         )
     mix_cols[me] = mix_parts[me]
-    norm_there = [0] + norm_ring.advance()
+    norm_there += norm_ring.advance()
     for i in range(model_width // deep):
         piece = slice(i * deep, (i + 1) * deep)
         rows_t[piece] = rows[:, :, piece].reshape(pairs, deep).astype(F32).T.astype(BF16)
     hidden_t[...] = hidden_ref[...].astype(F32).T.astype(BF16)
     save(rows_t, rows_t_hbm)
-    save(hidden_t, hidden_t_hbm)
+    for i in range(n_tp):
+        piece = slice(i * width, (i + 1) * width)
+        wd[:, piece] = mm(hidden_t[...], sent[:, :, piece].reshape(pairs, width)).astype(BF16)
+    save(wd, down_hbm)
     for d in range(1, n_sp):
         src_span = at.span_back(d)
         landed(later_in.at[src_span], later_recv.at[src_span])
@@ -743,6 +753,10 @@
     decay_grad = mm(lower, moved, 0, 0, precision=HIGHEST) + final
     dstep_ref[...] = (stepped - rate_ref[...] * decay_grad).T
 
+    save(dx_ref, dx_hbm)
+    save(db_ref, db_hbm)
+    save(dstep_ref, dstep_hbm)
+
     for d in range(1, n_sp):
         src_span = at.span_back(d)
         block = mix_cols.at[src_span, stripe(t)]
@@ -771,6 +785,7 @@
         if not norm_ring.more():
             break
         norm_there = norm_ring.advance()
+    save(proj_ref, proj_hbm)
     for wait in waits:
         wait()
     for copy in saves:
@@ -810,8 +825,7 @@
         functools.partial(main_kernel, n_sp, n_tp),
         out_shape=(
             out((model_width, pairs), BF16),
-            out((n_sp, capacity, model_width), BF16),
-            out((units, pairs), BF16),
+            out((units, model_width), BF16),
             out((pairs, units), BF16),
             out((pairs, units), BF16),
             out((channels, out_columns), F32),
@@ -822,8 +836,14 @@
             out(x.shape, BF16),
         ),
         in_specs=whole(4) + [anywhere] * 3 + whole(len(args) - 7),
-        out_specs=tuple([anywhere] * 5 + whole(6)),
+        out_specs=tuple([anywhere] * 10),
         scratch_shapes=[
+            full(channels, out_columns),
+            low(*x.shape),
+            full(*step.shape),
+            low(*b_rows.shape),
+            low(*c_rows.shape),
+            low(*x.shape),
             low(n_sp, capacity, model_width),
             low(n_sp, capacity, model_width),
             low(model_width, pairs),
@@ -846,7 +866,7 @@
             DMA((n_sp,)),
             DMA((n_sp,)),
             DMA((n_sp,)),
-            DMA((5,)),
+            DMA((10,)),
             low(model_width, units),
             low(model_width, units),
             low(units, model_width),
@@ -912,20 +932,17 @@
     )(*args)
 
 
-def weight_grad_kernel(count, rows_ref, hidden_ref, sent_ref, gate_ref, up_ref, *rest):
-    ready, (g_out, u_out, d_out), out = rest[:count], rest[count : count + 3], rest[count + 3 :]
-    capacity = sent_ref.shape[1]
-    sent = sent_ref[...].reshape(sent_ref.shape[0] * capacity, sent_ref.shape[2])
+def weight_grad_kernel(count, rows_ref, gate_ref, up_ref, *rest):
+    ready, (g_out, u_out), out = rest[:count], rest[count : count + 2], rest[count + 2 :]
     g_out[...] = mm(rows_ref[...], gate_ref[...]).astype(BF16)
     u_out[...] = mm(rows_ref[...], up_ref[...]).astype(BF16)
-    d_out[...] = mm(hidden_ref[...], sent).astype(BF16)
     for source, target in zip(ready, out):
         target[...] = source[...]
 
 
-def expert_weight_grads(rows_t, sent, hidden_t, gate_grad, up_grad, ready):
+def expert_weight_grads(rows_t, gate_grad, up_grad, ready):
     model_width, pairs = rows_t.shape
-    units = hidden_t.shape[0]
+    units = gate_grad.shape[1]
     tile = 512
     steps = model_width // tile
     fixed = pl.BlockSpec((pairs, units), lambda i: (0, 0))
@@ -942,20 +959,17 @@
         out_shape=(
             jax.ShapeDtypeStruct((model_width, units), BF16),
             jax.ShapeDtypeStruct((model_width, units), BF16),
-            jax.ShapeDtypeStruct((units, model_width), BF16),
             *(jax.ShapeDtypeStruct(array.shape, array.dtype) for array in ready),
         ),
         in_specs=[
             pl.BlockSpec((tile, pairs), lambda i: (i, 0)),
-            pl.BlockSpec((units, pairs), lambda i: (0, 0)),
-            pl.BlockSpec(sent.shape[:2] + (tile,), lambda i: (0, 0, i)),
             fixed,
             fixed,
             *handed,
         ],
-        out_specs=(tall, tall, pl.BlockSpec((units, tile), lambda i: (0, i)), *handed),
+        out_specs=(tall, tall, *handed),
         name="expert_weight_grads",
-    )(rows_t, hidden_t, sent, gate_grad, up_grad, *ready)
+    )(rows_t, gate_grad, up_grad, *ready)
 
 
 def body(
@@ -978,7 +992,7 @@
     mixer_output_weight,
 ):
     n_sp, n_tp = lax.axis_size("sp"), lax.axis_size("tp")
-    rows_t, sent, hidden_t, gate_grad, up_grad, *ready = main_part(
+    rows_t, grad_d, gate_grad, up_grad, *ready = main_part(
         mixer_output_stream,
         layer_output_gradient,
         routes.T,
@@ -1000,7 +1014,7 @@
         n_tp,
     )
     grad_g, grad_u, grad_d, proj_grad, input_grad, step_grad, b_grad, c_grad, gate_grad_in = (
-        expert_weight_grads(rows_t, sent, hidden_t, gate_grad, up_grad, ready)
+        expert_weight_grads(rows_t, gate_grad, up_grad, [grad_d, *ready])
     )
     return (
         grad_g[None],

time: 146 us -> 145 us (level)
  no operation moved by 1% of the time
where the time goes in v1:
time: 145 us
  Pallas kernels  144 us (99%)
    pallas_call x1, Pallas kernels, main_part(): pl.pallas_call(functools.partial(main_kernel, n_sp, n_tp), out_shape=(out...  133 us
    pallas_call x1, Pallas kernels, expert_weight_grads(): pl.pallas_call(functools.partial(weight_grad_kernel, len(ready)), grid=(s...  10.4 us

profile of v1, /device:TPU:0, one launch (start us, length us, event | category | flops | bytes accessed | tf_op | source)
XLA Modules:
  0.0 144.6 jit_solution(10343501292466478635)
XLA Ops:
  0.6 133.4 %main_part.1 = (bf16[2048,384]{1,0:T(8,128)(2,1)}, bf16[896,2048]{1,0:T(8,128)(2,1)}, bf16[384,896]{1,0:T(8,128)(2,1)}, bf16[384,896]{1,0:T(8,128)(2,1)}, f32[10...) custom-call(bf16[128,512]{1,0:T(8,128)(2,1)} %stream_ref.1, ...), custom_call_target="tpu_custom_call" | custom-call | tf_op jit(solution)/shard_map/main_part/pallas_call | solution.py:824
  134.1 10.4 %expert_weight_grads.1 = (bf16[2048,896]{1,0:T(8,128)(2,1)}, bf16[2048,896]{1,0:T(8,128)(2,1)}, bf16[896,2048]{1,0:T(8,128)(2,1)}, f32[1024,256]{1,0:T(8,128)}, ...) custom-call(bf16[2048,384]{1,0:T(8,128)(2,1)} %get-tuple-element.28., ...), custom_call_target="tpu_custom_call" | custom-call | tf_op jit(solution)/shard_map/expert_weight_grads/pallas_call | solution.py:956
